TPU v7x, 512 devices: a whole 4x8x8 slice. The times are simulated.
512 devices in a mesh: fs: 64 (over z, y), tp: 8 (over x, core).
Axes of the slice: x: 4, y: 8, z: 8, core: 2. Of those that a mesh axis runs over, the one named last changes fastest.
Arguments:
- inputs: bfloat16 [32768, 2048], P('fs', 'tp'), may hold values from -6 to 6
- hidden_pre: bfloat16 [32768, 4096], P('fs', 'tp'), may hold values from -6 to 6
- norm_input: bfloat16 [32768, 2048], P('fs', 'tp'), may hold values from -48 to 48, as said below
- out_gain: float32 [2048], P('tp'), may hold values from 0.1 to 1.9
- w_up: bfloat16 [2048, 4096], P('tp', 'fs'), may hold values from -0.125 to 0.125
- w_down: bfloat16 [4096, 2048], P('tp', 'fs'), may hold values from -0.09375 to 0.09375
- cotangent: bfloat16 [32768, 2048], P('fs', 'tp'), may hold values from -16 to 16
Outputs:
- grad_input: bfloat16 [32768, 2048], P('fs', 'tp')
- grad_up: float32 [2048, 4096], P('tp', 'fs')
- grad_gain: float32 [2048], P('tp')
Inputs may be any that keep to these rules, and one draw needn't show every extreme that they name: `norm_input`: each token's features are scaled by a factor of that token, and each block of 2048 / 8 features by a factor of that block.
All inputs are finite; a program needn't handle non-finite values.
Results may differ from a plain program's by a relative error of at most 0.0058.
Values may be sent and summed in bfloat16 or wider, within the bound.
No kernel may reach another device: no remote copies, remote signals or barrier semaphores. Data moves between devices by JAX's collectives and lax.ppermute only.
A program may use at most 64 MiB of HBM per device.

v0:
```python
import jax
import jax.numpy as jnp
from jax import lax
from jax.sharding import Mesh
from jax.sharding import PartitionSpec as P

FS = ("fs_0", "fs_1")
norm_eps = 1e-06


def from_everyone(value, axis):
    devices = lax.axis_size(axis)
    return lax.all_to_all(
        jnp.broadcast_to(value[None], (devices, *value.shape)), axis, 0, 0, tiled=True
    )


def taken_together(value, axis):
    everything = from_everyone(value, axis)
    return jnp.sum(everything, axis=0)


def in_one(arrays, axis):
    ends = [0]
    for a in arrays:
        ends.append(ends[-1] + a.size)
    total = taken_together(jnp.concatenate([a.ravel() for a in arrays]), axis)
    return tuple((total[b:e].reshape(a.shape) for a, b, e in zip(arrays, ends, ends[1:])))


def one_axis_at_a_time(value, axes):
    for axis in axes:
        value = lax.psum(value, axis)
    return value


def joined_along(parts, dim):
    parts = jnp.moveaxis(parts, 0, dim)
    dims = parts.shape
    return parts.reshape(*dims[:dim], dims[dim] * dims[dim + 1], *dims[dim + 2 :])


def gather_directly(value, axis, dim):
    parts = from_everyone(value, axis)
    return joined_along(parts, dim)


def stacked_from(value, axes, order):
    parts = value[None]
    for k in order:
        parts = lax.all_gather(parts, axes[k], axis=0, tiled=True)
    block = [lax.axis_size(axes[k]) for k in reversed(order)]
    parts = parts.reshape(*block, *value.shape)
    turned = sorted(range(len(order)), key=lambda place: order[len(order) - 1 - place])
    return parts.transpose(*turned, *range(len(order), parts.ndim)).reshape(-1, *value.shape)


def gather_axes(value, axes, order, dim):
    return joined_along(stacked_from(value, axes, order), dim)


def summed_rows(value, axes, dim):
    for axis in axes:
        value = lax.psum_scatter(value, axis, scatter_dimension=dim, tiled=True)
    return value


def on_device(inputs, hidden_pre, norm_input, out_gain, w_up, w_down, cotangent):
    tok_rows = inputs.shape[0]
    width = inputs.shape[1] * lax.axis_size("tp")
    scaled = (tok_rows * lax.axis_size(FS)) ** (-0.5)
    normed = norm_input.astype(jnp.float32)
    upstream = cotangent.astype(jnp.float32)
    weighted = upstream * out_gain
    square_sum, cross_sum = in_one(
        (jnp.sum(normed * normed, axis=1), jnp.sum(weighted * normed, axis=1)), "tp"
    )
    inv_rms = lax.rsqrt(square_sum / width + norm_eps)[:, None]
    cross_mean = (cross_sum / width)[:, None]
    d_out = (weighted * inv_rms - normed * inv_rms * inv_rms * inv_rms * cross_mean).astype(
        jnp.bfloat16
    )
    grad_gain = one_axis_at_a_time(jnp.sum(upstream * normed * inv_rms, axis=0) * scaled, FS)
    out_full = gather_directly(d_out, "tp", 1)
    columns = out_full
    d_act = lax.dot_general(
        columns,
        gather_axes(w_down, FS, (0, 1), 1),
        (((1,), (1,)), ((), ())),
        preferred_element_type=jnp.float32,
    )
    d_pre = (d_act * 2.0 * jax.nn.relu(hidden_pre.astype(jnp.float32))).astype(jnp.bfloat16)
    hidden_full = lax.all_gather(d_pre, "tp", axis=1, tiled=True)
    columns = hidden_full
    grad_input = lax.dot_general(
        columns,
        lax.all_gather(w_up, FS, axis=1, tiled=True),
        (((1,), (1,)), ((), ())),
        preferred_element_type=jnp.float32,
    ).astype(jnp.bfloat16)
    whole_term = (
        lax.dot_general(
            hidden_full, inputs, (((0,), (0,)), ((), ())), preferred_element_type=jnp.float32
        )
        * scaled
    )
    grad_up = summed_rows(whole_term, FS, 0).T
    return (grad_input, grad_up, grad_gain)


def solution(mesh):
    torus = Mesh(mesh.devices.reshape(8, 8, mesh.shape["tp"]), ("fs_0", "fs_1", "tp"))
    in_specs = (
        P(FS, "tp"),
        P(FS, "tp"),
        P(FS, "tp"),
        P("tp"),
        P("tp", FS),
        P("tp", FS),
        P(FS, "tp"),
    )
    out_specs = (P(FS, "tp"), P("tp", FS), P("tp"))
    return jax.shard_map(
        on_device, mesh=torus, in_specs=in_specs, out_specs=out_specs, check_vma=False
    )
```

profile of v0, /device:TPU:6, one launch (start us, length us, event | category | flops | bytes accessed | tf_op | source)
XLA Modules:
  0.0 246.0 jit_solution(17596367826111091204)
XLA Ops:
  8.0 0.0 copy-start
  8.0 0.0 all-gather.5.cloned.1.call-start
  8.1 31.5 %all-gather = bf16[4096,32]{0,1:T(8,128)(2,1)S(1)} all-gather(bf16[512,32]{0,1:T(8,128)(2,1)} %param.12), channel_id=2, replica_groups=mesh['fs_0'=8,'fs_1'=8,'tp'=8] {'fs_0'}, dimensions={0}, use_global_device_ids=true | all-gather | bytes 294912 | tf_op jit(solution)/shard_map/all_gather | solution.py:51
  39.5 0.8 copy.27
  40.3 0.0 all-gather.5.cloned.1.call-update
  40.4 1.3 fusion.5
  41.7 8.0 %all_to_all.11 = f32[8,1,1024]{2,1,0:T(1,128)S(1)} all-to-all(f32[8,1,1024]{2,1,0:T(1,128)S(1)} %broadcast_in_dim.6), channel_id=1, replica_groups=mesh['fs_0'=8,'fs_1'=8,'tp'=8] {'tp'}, dimensions={0} | all-to-all | bytes 65536 | tf_op jit(solution)/shard_map/all_to_all | solution.py:13
  49.7 1.3 fusion.11
  51.0 0.1 copy.20
  51.1 1.5 broadcast_in_dim.7
  52.6 5.6 %all-to-all-start.1 = ((bf16[8,512,256]{1,2,0:T(8,128)(2,1)}), bf16[8,512,256]{1,2,0:T(8,128)(2,1)S(1)}, u32[]{:S(2)}, u32[]{:S(2)}) async-start(bf16[8,512,256]{1,2,0:T(8,128)(2,1)} %broadcast_in_dim.7), calls=%async_computation.1 | async-start | bytes 4194304 | tf_op jit(solution)/shard_map/all_to_all | solution.py:13
  58.2 0.0 all-gather.7.cloned.1.call-start
  58.2 24.0 %all-gather.5.cloned.1.call-done = bf16[64,512,32]{1,0,2:T(8,128)(2,1)} async-done(((bf16[8,512,32]{1,0,2:T(8,128)(2,1)}), bf16[64,512,32]{1,0,2:T(8,128)(2,1)}) %all-gather.5.cloned.1.call-update) | async-done | bytes 2097168 | tf_op jit(solution)/shard_map/all_gather | solution.py:51
  82.2 4.2 %copy.22 = bf16[8,8,512,32]{2,3,1,0:T(8,128)(2,1)} copy(bf16[8,8,512,32]{2,0,1,3:T(8,128)(2,1)} %bitcast.22) | data formatting | bytes 4194304 | tf_op jit(solution)/shard_map/transpose | solution.py:55
  86.4 0.0 all-to-all-done.1
  86.4 0.0 copy-done.1
  86.4 3.7 %fusion.1 = bf16[512,512]{1,0:T(8,128)(2,1)} fusion(bf16[512,2048]{0,1:T(8,128)(2,1)S(1)} %bitcast.23, bf16[512,2048]{0,1:T(8,128)(2,1)} %bitcast.24, bf16[512,512]{1,0:T(8,128)(2,1)S(1)} %copy-done.1), kind=kOutput, calls=%fused_computation.3 | convolution fusion | flops 1075052544 | bytes 5242880 | tf_op jit(solution)/shard_map/dot_general | solution.py:86
  90.1 0.0 all-gather.7.cloned.1.call-update
  90.1 0.0 reduce-scatter.3.cloned.1.call-start
  90.2 34.4 %all-gather.7.cloned.1.call-done = bf16[512,4096]{1,0:T(8,128)(2,1)} async-done(((bf16[512,512]{1,0:T(8,128)(2,1)}), bf16[512,4096]{1,0:T(8,128)(2,1)}) %all-gather.7.cloned.1.call-update) | async-done | bytes 4194320 | tf_op jit(solution)/shard_map/all_gather | solution.py:93
  124.6 0.0 copy-done
  124.6 5.4 %convolution_multiply_fusion = f32[4096,256]{1,0:T(8,128)} fusion(bf16[512,4096]{1,0:T(8,128)(2,1)} %all-gather.7.cloned.1.call-done, bf16[512,256]{1,0:T(8,128)(2,1)S(1)} %copy-done), kind=kOutput, calls=%fused_computation | convolution fusion | flops 1074790400 | bytes 8650752 | tf_op jit(solution)/shard_map/dot_general | solution.py:102
  130.0 0.0 reduce-scatter.3.cloned.1.call-update
  130.0 0.0 all-gather.9.cloned.1.call-start
  130.1 0.5 all-gather.9.cloned.1.call-update
  130.6 0.0 reduce-scatter.5.cloned.1.call-start
  130.7 61.3 %reduce-scatter.3.cloned.1.call-done = f32[512,256]{1,0:T(8,128)} async-done(((f32[4096,256]{1,0:T(8,128)}), f32[512,256]{1,0:T(8,128)}) %reduce-scatter.3.cloned.1.call-update) | async-done | bytes 524304 | tf_op jit(solution)/shard_map/reduce_scatter | solution.py:64
  192.0 0.0 reduce-scatter.5.cloned.1.call-update
  192.0 15.4 %psum.14 = f32[256]{0:T(256)S(1)} all-reduce(f32[256]{0:T(256)S(1)} %broadcast_multiply_fusion), channel_id=1, replica_groups=mesh['fs_0'=8,'fs_1'=8,'tp'=8] {'fs_0'}, use_global_device_ids=true, to_apply=%region_6.7 | all-reduce | flops 256 | bytes 2048 | tf_op jit(solution)/shard_map/psum | solution.py:33
  207.4 17.6 %psum.15 = f32[256]{0:T(256)} all-reduce(f32[256]{0:T(256)S(1)} %psum.14), channel_id=1, replica_groups=mesh['fs_0'=8,'fs_1'=8,'tp'=8] {'fs_1'}, use_global_device_ids=true, to_apply=%region_7.8 | all-reduce | flops 256 | bytes 2048 | tf_op jit(solution)/shard_map/psum | solution.py:33
  225.1 9.0 %all-gather.9.cloned.1.call-done = bf16[256,4096]{0,1:T(8,128)(2,1)} async-done(((bf16[256,64]{0,1:T(8,128)(2,1)}), bf16[256,4096]{0,1:T(8,128)(2,1)}) %all-gather.9.cloned.1.call-update) | async-done | bytes 2097168 | tf_op jit(solution)/shard_map/all_gather | solution.py:97
  234.1 4.8 %convolution_convert_fusion = bf16[512,256]{1,0:T(8,128)(2,1)} fusion(bf16[512,4096]{1,0:T(8,128)(2,1)} %all-gather.7.cloned.1.call-done, bf16[256,4096]{0,1:T(8,128)(2,1)} %all-gather.9.cloned.1.call-done), kind=kOutput, calls=%fused_computation.4 | convolution fusion | flops 1073872896 | bytes 6553600 | tf_op jit(solution)/shard_map/dot_general | solution.py:95
  (7 shorter events, 0.1 us)
Async XLA Ops:
  8.0 116.6 %copy-start = (bf16[512,256]{1,0:T(8,128)(2,1)S(1)}, bf16[512,256]{1,0:T(8,128)(2,1)}, u32[]{:S(2)}) copy-start(bf16[512,256]{1,0:T(8,128)(2,1)} %param.7) | copy-start | bytes 786436
  8.0 74.2 %all-gather.5.cloned.1.call-start = ((), (), s32[]{:S(2)}) async-start(), calls=%async_computation.4 | async-start | bytes 2359296 | tf_op jit(solution)/shard_map/all_gather | solution.py:51
  52.6 33.8 %all-to-all-start.1 = ((bf16[8,512,256]{1,2,0:T(8,128)(2,1)}), bf16[8,512,256]{1,2,0:T(8,128)(2,1)S(1)}, u32[]{:S(2)}, u32[]{:S(2)}) async-start(bf16[8,512,256]{1,2,0:T(8,128)(2,1)} %broadcast_in_dim.7), calls=%async_computation.1 | async-start | bytes 4194304 | tf_op jit(solution)/shard_map/all_to_all | solution.py:13
  58.2 66.3 %all-gather.7.cloned.1.call-start = ((), (), s32[]{:S(2)}) async-start(), calls=%async_computation.5 | async-start | bytes 4718592 | tf_op jit(solution)/shard_map/all_gather | solution.py:93
  82.2 4.2 %copy-start.1 = (bf16[512,512]{1,0:T(8,128)(2,1)S(1)}, bf16[512,512]{1,0:T(8,128)(2,1)}, u32[]{:S(2)}) copy-start(bf16[512,512]{1,0:T(8,128)(2,1)} %param.8) | copy-start | bytes 1572868
  90.1 101.9 %reduce-scatter.3.cloned.1.call-start = ((), (), s32[]{:S(2)}) async-start(), calls=%async_computation.7 | async-start | bytes 4718592 | tf_op jit(solution)/shard_map/reduce_scatter | solution.py:64
  130.0 104.0 %all-gather.9.cloned.1.call-start = ((), (), s32[]{:S(2)}) async-start(), calls=%async_computation.6 | async-start | bytes 2129920 | tf_op jit(solution)/shard_map/all_gather | solution.py:97
  130.6 108.3 %reduce-scatter.5.cloned.1.call-start = ((), (), s32[]{:S(2)}) async-start(), calls=%async_computation.8 | async-start | bytes 589824 | tf_op jit(solution)/shard_map/reduce_scatter | solution.py:64
Sparse Core Ops, SparseCore 0:
  40.5 41.7 all-gather.4
  90.2 34.2 all-gather.6
  130.1 61.7 reduce-scatter.2
  195.2 38.8 reduce-scatter.4
Sparse Core Ops, SparseCore 1:
  133.6 100.4 all-gather.8
where the time goes:
time: 246 us
  waiting for transfers between devices  129 us (52%)
  blocking collectives  72.5 us (29%)
  between operations  15.3 us (6%)
  matrix products  13.9 us (6%)
  local copies, waits for them, and re-layouts  6.63 us (3%)
  starting transfers between devices  5.77 us (2%)
  other arithmetic  2.63 us (1%)
    reduce_scatter x2, waiting for transfers between devices, summed_rows(): value = lax.psum_scatter(value, axis, scatter_dimension=dim, tiled=True)  61.3 us
    all_gather x1, waiting for transfers between devices, on_device(): hidden_full = lax.all_gather(d_pre, 'tp', axis=1, tiled=True)  34.4 us
    psum x2, blocking collectives, one_axis_at_a_time(): value = lax.psum(value, axis)  33.1 us
    all_gather x1, blocking collectives, stacked_from(): parts = lax.all_gather(parts, axes[k], axis=0, tiled=True)  31.5 us
    all_gather x1, waiting for transfers between devices, stacked_from(): parts = lax.all_gather(parts, axes[k], axis=0, tiled=True)  24 us
    all_gather x1, waiting for transfers between devices, on_device(): lax.all_gather(w_up, FS, axis=1, tiled=True)  9 us
    all_to_all x1, blocking collectives, from_everyone(): lax.all_to_all(jnp.broadcast_to(value[None], (devices, *value.shape)), ax...  7.95 us
    all_to_all x1, starting transfers between devices, from_everyone(): lax.all_to_all(jnp.broadcast_to(value[None], (devices, *value.shape)), ax...  5.61 us
  transfers between devices with their start and end apart: 6, of which 4 were waited for; matrix products, arithmetic and copies ran while one was open for 5% of the time, Pallas kernels for 0%

commit v1 on v0

--- a/solution.py
+++ b/solution.py
@@ -90,7 +90,9 @@
         preferred_element_type=jnp.float32,
     )
     d_pre = (d_act * 2.0 * jax.nn.relu(hidden_pre.astype(jnp.float32))).astype(jnp.bfloat16)
-    hidden_full = lax.all_gather(d_pre, "tp", axis=1, tiled=True)
+    hidden_full = jnp.concatenate(
+        lax.all_to_all(jnp.stack([d_pre] * lax.axis_size("tp")), "tp", 0, 0), axis=1
+    )
     columns = hidden_full
     grad_input = lax.dot_general(
         columns,

time: 246 us -> 260 us (1.057)
  blocking collectives: 72.5 us -> 125 us
  waiting for transfers between devices: 129 us -> 90.9 us
  matrix products: 13.9 us -> 11 us
    all_to_all x0 -> x1, blocking collectives: none -> 52.2 us  [on_device(): lax.all_to_all(jnp.stack([d_pre] * lax.axis_size('tp')), 'tp', 0, 0)]
    all_gather x1 -> x0, waiting for transfers between devices: 34.4 us -> none  [on_device(): hidden_full = lax.all_gather(d_pre, 'tp', axis=1, tiled=True)]
    reduce_scatter x2, waiting for transfers between devices: 61.3 us -> 57.9 us  [summed_rows(): value = lax.psum_scatter(value, axis, scatter_dimension=dim, tiled=True)]
  transfers between devices with their start and end apart: 6 -> 5, of which waited for: 4 -> 3; matrix products, arithmetic and copies ran while one was open for 5% -> 5% of each run, Pallas kernels for 0% -> 0%
where the time goes in v1:
time: 260 us; the launch traced here: 259 us
  blocking collectives  125 us (48%)
  waiting for transfers between devices  90.9 us (35%)
  between operations  15.3 us (6%)
  matrix products  11 us (4%)
  local copies, waits for them, and re-layouts  9.06 us (3%)
  starting transfers between devices  5.73 us (2%)
  other arithmetic  2.63 us (1%)
    reduce_scatter x2, waiting for transfers between devices, summed_rows(): value = lax.psum_scatter(value, axis, scatter_dimension=dim, tiled=True)  57.9 us
    all_to_all x1, blocking collectives, on_device(): lax.all_to_all(jnp.stack([d_pre] * lax.axis_size('tp')), 'tp', 0, 0)  52.2 us
    psum x2, blocking collectives, one_axis_at_a_time(): value = lax.psum(value, axis)  33.1 us
    all_gather x1, blocking collectives, stacked_from(): parts = lax.all_gather(parts, axes[k], axis=0, tiled=True)  31.5 us
    all_gather x1, waiting for transfers between devices, stacked_from(): parts = lax.all_gather(parts, axes[k], axis=0, tiled=True)  24 us
    all_gather x1, waiting for transfers between devices, on_device(): lax.all_gather(w_up, FS, axis=1, tiled=True)  8.42 us
    all_to_all x1, blocking collectives, from_everyone(): lax.all_to_all(jnp.broadcast_to(value[None], (devices, *value.shape)), ax...  7.95 us
    all_to_all x1, starting transfers between devices, from_everyone(): lax.all_to_all(jnp.broadcast_to(value[None], (devices, *value.shape)), ax...  5.61 us
  transfers between devices with their start and end apart: 5, of which 3 were waited for; matrix products, arithmetic and copies ran while one was open for 5% of the time, Pallas kernels for 0%

profile of v1, /device:TPU:6, one launch (start us, length us, event | category | flops | bytes accessed | tf_op | source)
XLA Modules:
  0.0 259.3 jit_solution(5526118361526320037)
XLA Ops:
  8.0 0.0 copy-start
  8.0 0.0 all-gather.4.cloned.1.call-start
  8.1 31.5 %all-gather = bf16[4096,32]{0,1:T(8,128)(2,1)S(1)} all-gather(bf16[512,32]{0,1:T(8,128)(2,1)} %param.12), channel_id=2, replica_groups=mesh['fs_0'=8,'fs_1'=8,'tp'=8] {'fs_0'}, dimensions={0}, use_global_device_ids=true | all-gather | bytes 294912 | tf_op jit(solution)/shard_map/all_gather | solution.py:51
  39.5 0.8 copy.32
  40.3 0.0 all-gather.4.cloned.1.call-update
  40.4 1.3 fusion.5
  41.7 8.0 %all_to_all.16 = f32[8,1,1024]{2,1,0:T(1,128)S(1)} all-to-all(f32[8,1,1024]{2,1,0:T(1,128)S(1)} %broadcast_in_dim.6), channel_id=1, replica_groups=mesh['fs_0'=8,'fs_1'=8,'tp'=8] {'tp'}, dimensions={0} | all-to-all | bytes 65536 | tf_op jit(solution)/shard_map/all_to_all | solution.py:13
  49.7 1.3 fusion.11
  51.0 0.1 copy.24
  51.1 1.5 broadcast_in_dim.7
  52.6 5.6 %all-to-all-start.1 = ((bf16[8,512,256]{1,2,0:T(8,128)(2,1)}), bf16[8,512,256]{1,2,0:T(8,128)(2,1)S(1)}, u32[]{:S(2)}, u32[]{:S(2)}) async-start(bf16[8,512,256]{1,2,0:T(8,128)(2,1)} %broadcast_in_dim.7), calls=%async_computation.1 | async-start | bytes 4194304 | tf_op jit(solution)/shard_map/all_to_all | solution.py:13
  58.2 0.0 reduce-scatter.3.cloned.1.call-start
  58.2 24.0 %all-gather.4.cloned.1.call-done = bf16[64,512,32]{1,0,2:T(8,128)(2,1)} async-done(((bf16[8,512,32]{1,0,2:T(8,128)(2,1)}), bf16[64,512,32]{1,0,2:T(8,128)(2,1)}) %all-gather.4.cloned.1.call-update) | async-done | bytes 2097168 | tf_op jit(solution)/shard_map/all_gather | solution.py:51
  82.2 4.1 %copy.26 = bf16[8,8,512,32]{2,3,1,0:T(8,128)(2,1)} copy(bf16[8,8,512,32]{2,0,1,3:T(8,128)(2,1)} %bitcast.27) | data formatting | bytes 4194304 | tf_op jit(solution)/shard_map/transpose | solution.py:55
  86.4 0.0 all-to-all-done.1
  86.4 0.0 copy-done.2
  86.4 2.9 %fusion.1 = bf16[512,512]{1,0:T(8,128)(2,1)S(1)} fusion(bf16[512,2048]{0,1:T(8,128)(2,1)S(1)} %bitcast.28, bf16[512,2048]{0,1:T(8,128)(2,1)} %bitcast.29, bf16[512,512]{1,0:T(8,128)(2,1)S(1)} %copy-done.2), kind=kOutput, calls=%fused_computation.3 | convolution fusion | flops 1075052544 | bytes 5242880 | tf_op jit(solution)/shard_map/dot_general | solution.py:86
  89.3 0.2 copy.27
  89.5 0.4 stack.2
  89.9 52.2 %all_to_all.17 = bf16[8,512,512]{1,2,0:T(8,128)(2,1)S(1)} all-to-all(bf16[8,512,512]{1,2,0:T(8,128)(2,1)S(1)} %stack.2), channel_id=1, replica_groups=mesh['fs_0'=8,'fs_1'=8,'tp'=8] {'tp'}, dimensions={0} | all-to-all | bytes 8388608 | tf_op jit(solution)/shard_map/all_to_all | solution.py:94
  142.1 1.9 copy-done.1
  144.0 3.2 %convolution_multiply_fusion = f32[4096,256]{1,0:T(8,128)} fusion(bf16[512,4096]{0,1:T(8,128)(2,1)S(1)} %bitcast.25, bf16[512,256]{1,0:T(8,128)(2,1)S(1)} %copy-done), kind=kOutput, calls=%fused_computation | convolution fusion | flops 1074790400 | bytes 8650752 | tf_op jit(solution)/shard_map/dot_general | solution.py:104
  147.2 0.0 reduce-scatter.3.cloned.1.call-update
  147.2 0.0 all-gather.6.cloned.1.call-start
  147.3 0.5 all-gather.6.cloned.1.call-update
  147.8 0.0 reduce-scatter.5.cloned.1.call-start
  147.9 57.9 %reduce-scatter.3.cloned.1.call-done = f32[512,256]{1,0:T(8,128)} async-done(((f32[4096,256]{1,0:T(8,128)}), f32[512,256]{1,0:T(8,128)}) %reduce-scatter.3.cloned.1.call-update) | async-done | bytes 524304 | tf_op jit(solution)/shard_map/reduce_scatter | solution.py:64
  205.8 0.0 reduce-scatter.5.cloned.1.call-update
  205.8 15.4 %psum.14 = f32[256]{0:T(256)S(1)} all-reduce(f32[256]{0:T(256)S(1)} %broadcast_multiply_fusion), channel_id=1, replica_groups=mesh['fs_0'=8,'fs_1'=8,'tp'=8] {'fs_0'}, use_global_device_ids=true, to_apply=%region_6.7 | all-reduce | flops 256 | bytes 2048 | tf_op jit(solution)/shard_map/psum | solution.py:33
  221.3 17.6 %psum.15 = f32[256]{0:T(256)} all-reduce(f32[256]{0:T(256)S(1)} %psum.14), channel_id=1, replica_groups=mesh['fs_0'=8,'fs_1'=8,'tp'=8] {'fs_1'}, use_global_device_ids=true, to_apply=%region_7.8 | all-reduce | flops 256 | bytes 2048 | tf_op jit(solution)/shard_map/psum | solution.py:33
  238.9 8.4 %all-gather.6.cloned.1.call-done = bf16[256,4096]{0,1:T(8,128)(2,1)} async-done(((bf16[256,64]{0,1:T(8,128)(2,1)}), bf16[256,4096]{0,1:T(8,128)(2,1)}) %all-gather.6.cloned.1.call-update) | async-done | bytes 2097168 | tf_op jit(solution)/shard_map/all_gather | solution.py:99
  247.3 4.9 %convolution_convert_fusion = bf16[512,256]{1,0:T(8,128)(2,1)} fusion(bf16[512,4096]{0,1:T(8,128)(2,1)} %bitcast.26, bf16[256,4096]{0,1:T(8,128)(2,1)} %all-gather.6.cloned.1.call-done), kind=kOutput, calls=%fused_computation.4 | convolution fusion | flops 1073872896 | bytes 6553600 | tf_op jit(solution)/shard_map/dot_general | solution.py:97
  (9 shorter events, 0.1 us)
Async XLA Ops:
  8.0 136.0 %copy-start = (bf16[512,256]{1,0:T(8,128)(2,1)S(1)}, bf16[512,256]{1,0:T(8,128)(2,1)}, u32[]{:S(2)}) copy-start(bf16[512,256]{1,0:T(8,128)(2,1)} %param.7) | copy-start | bytes 786436
  8.0 74.2 %all-gather.4.cloned.1.call-start = ((), (), s32[]{:S(2)}) async-start(), calls=%async_computation.5 | async-start | bytes 2359296 | tf_op jit(solution)/shard_map/all_gather | solution.py:51
  52.6 33.8 %all-to-all-start.1 = ((bf16[8,512,256]{1,2,0:T(8,128)(2,1)}), bf16[8,512,256]{1,2,0:T(8,128)(2,1)S(1)}, u32[]{:S(2)}, u32[]{:S(2)}) async-start(bf16[8,512,256]{1,2,0:T(8,128)(2,1)} %broadcast_in_dim.7), calls=%async_computation.1 | async-start | bytes 4194304 | tf_op jit(solution)/shard_map/all_to_all | solution.py:13
  58.2 147.6 %reduce-scatter.3.cloned.1.call-start = ((), (), s32[]{:S(2)}) async-start(), calls=%async_computation.7 | async-start | bytes 4718592 | tf_op jit(solution)/shard_map/reduce_scatter | solution.py:64
  82.2 4.1 %copy-start.2 = (bf16[512,512]{1,0:T(8,128)(2,1)S(1)}, bf16[512,512]{1,0:T(8,128)(2,1)}, u32[]{:S(2)}) copy-start(bf16[512,512]{1,0:T(8,128)(2,1)} %param.8) | copy-start | bytes 1572868
  142.1 1.9 copy-start.1
  147.2 100.1 %all-gather.6.cloned.1.call-start = ((), (), s32[]{:S(2)}) async-start(), calls=%async_computation.6 | async-start | bytes 2129920 | tf_op jit(solution)/shard_map/all_gather | solution.py:99
  147.8 104.4 %reduce-scatter.5.cloned.1.call-start = ((), (), s32[]{:S(2)}) async-start(), calls=%async_computation.8 | async-start | bytes 589824 | tf_op jit(solution)/shard_map/reduce_scatter | solution.py:64
Sparse Core Ops, SparseCore 0:
  40.5 41.7 all-gather.3
  147.4 58.3 reduce-scatter.2
  209.2 38.7 reduce-scatter.4
Sparse Core Ops, SparseCore 1:
  150.8 96.5 all-gather.5
